TPU v7x, 32 devices: a whole 2x2x4 slice. The times are simulated.
32 devices in a mesh: fs: 8 (over z, y), tp: 4 (over x, core).
Axes of the slice: x: 2, y: 2, z: 4, core: 2. Of those that a mesh axis runs over, the one named last changes fastest.
Arguments:
- tokens: bfloat16 [8192, 2048], P('fs', 'tp'), may hold values from -6 to 6
- norm_gain: float32 [2048], P('fs'), may hold values from 0.1 to 1.9
- up_master: float32 [2048, 8192], P('fs', 'tp'), may hold values from -0.125 to 0.125
- down_master: float32 [2048, 8192], P('fs', 'tp'), may hold values from -0.0625 to 0.0625
Outputs:
- up_weights: bfloat16 [2048, 8192], P(None, 'tp')
- down_weights: bfloat16 [8192, 2048], P('tp')
- mlp_out: bfloat16 [8192, 2048], P('fs', 'tp')
All inputs are finite; a program needn't handle non-finite values.
Results may differ from a plain program's by a relative error of at most 0.014.
Values may be sent and summed in bfloat16 or wider, within the bound.
A program may use at most 128 MiB of HBM per device.

v0:
```python
import jax
import jax.numpy as jnp
from jax import lax
from jax.sharding import PartitionSpec as P

norm_floor = 1e-06


def on_device(tokens, norm_gain, up_master, down_master):
    up_local = (norm_gain[:, None] * up_master).astype(jnp.bfloat16)
    down_local = down_master.astype(jnp.bfloat16)
    gathered = lax.all_gather(tokens, "tp", axis=1, tiled=True)
    widened = gathered.astype(jnp.float32)
    normed = (
        widened * lax.rsqrt(jnp.mean(widened * widened, axis=-1, keepdims=True) + norm_floor)
    ).astype(jnp.bfloat16)
    up_whole, down_whole = (
        lax.all_gather(up_local, "fs", axis=0, tiled=True),
        lax.all_gather(down_local, "fs", axis=0, tiled=True),
    )
    preact = jnp.dot(normed, up_whole, preferred_element_type=jnp.float32)
    hidden = jnp.square(jax.nn.relu(preact)).astype(jnp.bfloat16)
    partial_value = jnp.einsum("tf,df->td", hidden, down_whole, preferred_element_type=jnp.float32)
    summed = lax.psum_scatter(
        partial_value.astype(jnp.bfloat16), "tp", scatter_dimension=1, tiled=True
    )
    return (up_whole, jnp.transpose(down_whole), summed)


def solution(mesh):
    in_specs = (P("fs", "tp"), P("fs"), P("fs", "tp"), P("fs", "tp"))
    out_specs = (P(None, "tp"), P("tp", None), P("fs", "tp"))
    return jax.shard_map(
        on_device, mesh=mesh, in_specs=in_specs, out_specs=out_specs, check_vma=False
    )
```

profile of v0, /device:TPU:0, one launch (start us, length us, event | category | flops | bytes accessed | tf_op | source)
XLA Modules:
  0.0 391.6 jit_solution(10137496696475460250)
XLA Ops:
  7.2 0.0 all-gather.8.cloned.1.call-start
  7.2 0.7 all-gather.8.cloned.1.call-update
  7.9 0.0 all-gather.4.cloned.1.call-start
  7.9 2.7 multiply_convert_fusion.1
  10.7 0.0 all-gather.4.cloned.1.call-update
  10.7 0.0 all-gather.6.cloned.1.call-start
  10.8 2.5 copy.7
  13.3 0.0 all-gather.6.cloned.1.call-update
  13.3 0.0 reduce-scatter.2.cloned.1.call-start
  13.4 33.4 %all-gather.8.cloned.1.call-done = bf16[1024,2048]{1,0:T(8,128)(2,1)} async-done(((bf16[1024,512]{1,0:T(8,128)(2,1)}), bf16[1024,2048]{1,0:T(8,128)(2,1)}) %all-gather.8.cloned.1.call-update) | async-done | bytes 4194320 | tf_op jit(solution)/shard_map/all_gather | solution.py:12
  46.7 3.1 fusion
  49.8 124.1 %all-gather.4.cloned.1.call-done = bf16[2048,2048]{1,0:T(8,128)(2,1)} async-done(((bf16[256,2048]{1,0:T(8,128)(2,1)}), bf16[2048,2048]{1,0:T(8,128)(2,1)}) %all-gather.4.cloned.1.call-update) | async-done | bytes 8388624 | tf_op jit(solution)/shard_map/all_gather | solution.py:18
  174.0 125.8 %all-gather.6.cloned.1.call-done = bf16[2048,2048]{0,1:T(8,128)(2,1)} async-done(((bf16[256,2048]{0,1:T(8,128)(2,1)}), bf16[2048,2048]{0,1:T(8,128)(2,1)}) %all-gather.6.cloned.1.call-update) | async-done | bytes 8388624 | tf_op jit(solution)/shard_map/all_gather | solution.py:19
  299.7 25.7 %fusion.9 = bf16[1024,2048]{1,0:T(8,128)(2,1)} fusion(bf16[2048,2048]{0,1:T(8,128)(2,1)} %all-gather.6.cloned.1.call-done, bf16[2048,2048]{1,0:T(8,128)(2,1)} %all-gather.4.cloned.1.call-done, bf16[1024,2048]{1,0:T(8,128)(2,1)} %all-gather.8.cloned.1.call-done, f32[1024]{0:T(1024)S(1)} %add_rsqrt_fusion), kind=kOutput, calls=%fused_computation.8 | convolution fusion | flops 17194549248 | bytes 25169920 | tf_op jit(solution)/shard_map/tf,df->td/dot_general | solution.py:23
  325.4 0.0 reduce-scatter.2.cloned.1.call-update
  325.5 42.7 %reduce-scatter.2.cloned.1.call-done = bf16[1024,512]{1,0:T(8,128)(2,1)} async-done(((bf16[1024,2048]{1,0:T(8,128)(2,1)}), bf16[1024,512]{1,0:T(8,128)(2,1)}) %reduce-scatter.2.cloned.1.call-update) | async-done | bytes 1048592 | tf_op jit(solution)/shard_map/reduce_scatter | solution.py:24
  368.2 8.4 %copy.10 = bf16[2048,2048]{1,0:T(8,128)(2,1)} copy(bf16[2048,2048]{1,0:T(8,128)(2,1)} %all-gather.4.cloned.1.call-done) | data formatting | bytes 16777216
  376.6 8.4 %copy.11 = bf16[2048,2048]{1,0:T(8,128)(2,1)} copy(bf16[2048,2048]{1,0:T(8,128)(2,1)} %bitcast.3) | data formatting | bytes 16777216
  (1 shorter events, 0.0 us)
Async XLA Ops:
  7.2 39.6 %all-gather.8.cloned.1.call-start = ((), (), s32[]{:S(2)}) async-start(), calls=%async_computation.3 | async-start | bytes 5242880 | tf_op jit(solution)/shard_map/all_gather | solution.py:12
  7.9 166.1 %all-gather.4.cloned.1.call-start = ((), (), s32[]{:S(2)}) async-start(), calls=%async_computation.1 | async-start | bytes 9437184 | tf_op jit(solution)/shard_map/all_gather | solution.py:18
  10.7 289.0 %all-gather.6.cloned.1.call-start = ((), (), s32[]{:S(2)}) async-start(), calls=%async_computation.2 | async-start | bytes 9437184 | tf_op jit(solution)/shard_map/all_gather | solution.py:19
  13.3 354.8 %reduce-scatter.2.cloned.1.call-start = ((), (), s32[]{:S(2)}) async-start(), calls=%async_computation.4 | async-start | bytes 5242880 | tf_op jit(solution)/shard_map/reduce_scatter | solution.py:24
Sparse Core Ops, SparseCore 0:
  9.5 37.1 all-gather.7
  49.4 124.4 all-gather.3
  176.6 123.1 all-gather.5
  325.6 42.5 reduce-scatter.1
where the time goes:
time: 392 us
  waiting for transfers between devices  327 us (83%)
  matrix products  25.7 us (7%)
  local copies, waits for them, and re-layouts  19.4 us (5%)
  between operations  13.8 us (4%)
  other arithmetic  5.82 us (1%)
    all_gather x1, waiting for transfers between devices, on_device(): lax.all_gather(down_local, 'fs', axis=0, tiled=True)  126 us
    all_gather x1, waiting for transfers between devices, on_device(): lax.all_gather(up_local, 'fs', axis=0, tiled=True)  124 us
    reduce_scatter x1, waiting for transfers between devices, on_device(): lax.psum_scatter(partial_value.astype(jnp.bfloat16), 'tp', scatter_dimens...  42.7 us
    all_gather x1, waiting for transfers between devices, on_device(): gathered = lax.all_gather(tokens, 'tp', axis=1, tiled=True)  33.4 us
    dot_general x1, matrix products, on_device(): jnp.einsum('tf,df->td', hidden, down_whole, preferred_element_type=jnp.fl...  25.7 us
    unnamed x3, local copies, waits for them, and re-layouts  19.4 us
  transfers between devices with their start and end apart: 4, of which 4 were waited for; matrix products, arithmetic and copies ran while one was open for 2% of the time, Pallas kernels for 0%

commit v1 on v0

--- a/solution.py
+++ b/solution.py
@@ -7,9 +7,17 @@
 
 
 def on_device(tokens, norm_gain, up_master, down_master):
+
+    def _answer_fields(field_in):
+        y2 = jnp.stack(tuple((field_in for _ in range(lax.axis_size("tp")))))
+        inter = jnp.concatenate(
+            lax.all_to_all(y2, axis_name="tp", split_axis=0, concat_axis=0), axis=1
+        )
+        return inter
+
     up_local = (norm_gain[:, None] * up_master).astype(jnp.bfloat16)
     down_local = down_master.astype(jnp.bfloat16)
-    gathered = lax.all_gather(tokens, "tp", axis=1, tiled=True)
+    gathered = _answer_fields(tokens)
     widened = gathered.astype(jnp.float32)
     normed = (
         widened * lax.rsqrt(jnp.mean(widened * widened, axis=-1, keepdims=True) + norm_floor)

time: 392 us -> 356 us (0.908)
  waiting for transfers between devices: 327 us -> 236 us
  blocking collectives: 0 us -> 52.2 us
    all_gather x1, waiting for transfers between devices: 124 us -> 67.7 us  [on_device(): lax.all_gather(up_local, 'fs', axis=0, tiled=True)]
    all_to_all x0 -> x1, blocking collectives: none -> 52.2 us  [_answer_fields(): lax.all_to_all(y2, axis_name='tp', split_axis=0, concat_axis=0)]
    all_gather x1 -> x0, waiting for transfers between devices: 33.4 us -> none  [on_device(): gathered = lax.all_gather(tokens, 'tp', axis=1, tiled=True)]
    unnamed x3 -> x6, local copies, waits for them, and re-layouts: 19.4 us -> 20 us
  transfers between devices with their start and end apart: 4 -> 3, of which waited for: 4 -> 3; matrix products, arithmetic and copies ran while one was open for 2% -> 2% of each run, Pallas kernels for 0% -> 0%
where the time goes in v1:
time: 356 us; the launch traced here: 355 us
  waiting for transfers between devices  236 us (66%)
  blocking collectives  52.2 us (15%)
  matrix products  25.6 us (7%)
  local copies, waits for them, and re-layouts  20.5 us (6%)
  between operations  13.8 us (4%)
  other arithmetic  7.03 us (2%)
    all_gather x1, waiting for transfers between devices, on_device(): lax.all_gather(down_local, 'fs', axis=0, tiled=True)  126 us
    all_gather x1, waiting for transfers between devices, on_device(): lax.all_gather(up_local, 'fs', axis=0, tiled=True)  67.7 us
    all_to_all x1, blocking collectives, _answer_fields(): lax.all_to_all(y2, axis_name='tp', split_axis=0, concat_axis=0)  52.2 us
    reduce_scatter x1, waiting for transfers between devices, on_device(): lax.psum_scatter(partial_value.astype(jnp.bfloat16), 'tp', scatter_dimens...  42.7 us
    dot_general x1, matrix products, on_device(): jnp.einsum('tf,df->td', hidden, down_whole, preferred_element_type=jnp.fl...  25.6 us
    unnamed x6, local copies, waits for them, and re-layouts  20 us
  transfers between devices with their start and end apart: 3, of which 3 were waited for; matrix products, arithmetic and copies ran while one was open for 2% of the time, Pallas kernels for 0%

profile of v1, /device:TPU:0, one launch (start us, length us, event | category | flops | bytes accessed | tf_op | source)
XLA Modules:
  0.0 355.4 jit_solution(15449002225518274749)
XLA Ops:
  7.2 0.0 copy-start
  7.2 0.0 all-gather.3.cloned.1.call-start
  7.2 2.8 multiply_convert_fusion.1
  10.0 0.0 all-gather.3.cloned.1.call-update
  10.1 0.0 all-gather.5.cloned.1.call-start
  10.1 2.5 copy.8
  12.7 0.0 all-gather.5.cloned.1.call-update
  12.7 0.0 reduce-scatter.2.cloned.1.call-start
  12.7 0.0 copy-done
  12.7 0.5 copy.9
  13.3 0.5 stack.2
  13.8 52.2 %all_to_all.5 = bf16[4,1024,512]{1,2,0:T(8,128)(2,1)S(1)} all-to-all(bf16[4,1024,512]{1,2,0:T(8,128)(2,1)S(1)} %stack.2), channel_id=1, replica_groups=mesh['fs'=8,'tp'=4] {'tp'}, dimensions={0} | all-to-all | bytes 8388608 | tf_op jit(solution)/shard_map/all_to_all | solution.py:14
  66.0 0.9 multiply_reduce_fusion
  66.9 3.3 fusion
  70.2 67.7 %all-gather.3.cloned.1.call-done = bf16[2048,2048]{1,0:T(8,128)(2,1)} async-done(((bf16[256,2048]{1,0:T(8,128)(2,1)}), bf16[2048,2048]{1,0:T(8,128)(2,1)}) %all-gather.3.cloned.1.call-update) | async-done | bytes 8388624 | tf_op jit(solution)/shard_map/all_gather | solution.py:26
  137.9 125.8 %all-gather.5.cloned.1.call-done = bf16[2048,2048]{0,1:T(8,128)(2,1)} async-done(((bf16[256,2048]{0,1:T(8,128)(2,1)}), bf16[2048,2048]{0,1:T(8,128)(2,1)}) %all-gather.5.cloned.1.call-update) | async-done | bytes 8388624 | tf_op jit(solution)/shard_map/all_gather | solution.py:27
  263.7 25.6 %fusion.3 = bf16[1024,2048]{1,0:T(8,128)(2,1)} fusion(bf16[2048,2048]{0,1:T(8,128)(2,1)} %all-gather.5.cloned.1.call-done, bf16[1024,2048]{0,1:T(8,128)(2,1)} %fusion, bf16[2048,2048]{1,0:T(8,128)(2,1)} %all-gather.3.cloned.1.call-done), kind=kOutput, calls=%fused_computation.6 | convolution fusion | flops 17188257792 | bytes 25165824 | tf_op jit(solution)/shard_map/tf,df->td/dot_general | solution.py:31
  289.2 0.0 reduce-scatter.2.cloned.1.call-update
  289.3 42.7 %reduce-scatter.2.cloned.1.call-done = bf16[1024,512]{1,0:T(8,128)(2,1)} async-done(((bf16[1024,2048]{1,0:T(8,128)(2,1)}), bf16[1024,512]{1,0:T(8,128)(2,1)}) %reduce-scatter.2.cloned.1.call-update) | async-done | bytes 1048592 | tf_op jit(solution)/shard_map/reduce_scatter | solution.py:32
  332.0 8.4 %copy.12 = bf16[2048,2048]{1,0:T(8,128)(2,1)} copy(bf16[2048,2048]{1,0:T(8,128)(2,1)} %all-gather.3.cloned.1.call-done) | data formatting | bytes 16777216
  340.4 8.4 %copy.13 = bf16[2048,2048]{1,0:T(8,128)(2,1)} copy(bf16[2048,2048]{1,0:T(8,128)(2,1)} %bitcast.10) | data formatting | bytes 16777216
  (1 shorter events, 0.0 us)
Async XLA Ops:
  7.2 5.6 %copy-start = (bf16[1024,512]{1,0:T(8,128)(2,1)S(1)}, bf16[1024,512]{1,0:T(8,128)(2,1)}, u32[]{:S(2)}) copy-start(bf16[1024,512]{1,0:T(8,128)(2,1)} %param.4) | copy-start | bytes 3145732
  7.2 130.7 %all-gather.3.cloned.1.call-start = ((), (), s32[]{:S(2)}) async-start(), calls=%async_computation.2 | async-start | bytes 9437184 | tf_op jit(solution)/shard_map/all_gather | solution.py:26
  10.1 253.6 %all-gather.5.cloned.1.call-start = ((), (), s32[]{:S(2)}) async-start(), calls=%async_computation.3 | async-start | bytes 9437184 | tf_op jit(solution)/shard_map/all_gather | solution.py:27
  12.7 319.3 %reduce-scatter.2.cloned.1.call-start = ((), (), s32[]{:S(2)}) async-start(), calls=%async_computation.4 | async-start | bytes 5242880 | tf_op jit(solution)/shard_map/reduce_scatter | solution.py:32
Sparse Core Ops, SparseCore 0:
  10.7 127.1 all-gather.2
  140.5 123.1 all-gather.4
  289.4 42.5 reduce-scatter.1
